TPU v7x, 32 devices: a whole 2x2x4 slice. The times are simulated.
32 devices in a mesh: ep: 8 (over z, y), tp: 4 (over x, core).
Axes of the slice: x: 2, y: 2, z: 4, core: 2. Of those that a mesh axis runs over, the one named last changes fastest.
Arguments:
- pool_input: bfloat16 [12288, 2048], P('ep', 'tp'), may hold values from -6 to 6
- group_mix: bfloat16 [4, 512, 512], P('tp'), may hold values from -0.25 to 0.25
- group_scale: float32 [2048], P('tp'), may hold values from 0.1 to 1.9
- out_proj: bfloat16 [2048, 2048], replicated, may hold values from -0.125 to 0.125
- moe_input: bfloat16 [4096, 2048], P(('ep', 'tp')), may hold values from -6 to 6
- norm_gain: float32 [2048], replicated, may hold values from 0.1 to 1.9
- expert_ids: int32 [4096, 2], P(('ep', 'tp')), may hold values from 0 to 31, all different within a row; in each aligned block of 128 rows (0 to 127, 128 to 255, ...) at most 16 rows name the same one
- expert_scores: float32 [4096, 2], P(('ep', 'tp')), may hold values from 0.1 to 1
- gate_proj: bfloat16 [32, 2048, 1024], P(('ep', 'tp')), may hold values from -0.125 to 0.125
- up_proj: bfloat16 [32, 2048, 1024], P(('ep', 'tp')), may hold values from -0.125 to 0.125
- down_proj: bfloat16 [32, 1024, 2048], P(('ep', 'tp')), may hold values from -0.1875 to 0.1875
Outputs:
- mixed_tokens: bfloat16 [12288, 2048], P(('ep', 'tp'))
- mixed_experts: bfloat16 [4096, 2048], P(('ep', 'tp'))
Inputs may be any that keep to these rules, and one draw needn't show every extreme that they name: `expert_ids`: each row names 2 different experts. Within the 128 rows of one device (aligned blocks) no expert is named by more than 16 rows, a bound that some block reaches of some device.
All inputs are finite; a program needn't handle non-finite values.
Results may differ from a plain program's by a relative error of at most 0.012.
Values may be sent and summed in bfloat16 or wider, within the bound.
A program may use at most 128 MiB of HBM per device.

v0:
```python
import jax
import jax.numpy as jnp
from jax import lax
from jax.sharding import PartitionSpec as P

epsilon = 1e-06


def shifted(value, axis, steps):
    count = lax.axis_size(axis)
    first, last = (max(0, -steps), min(count, count - steps))
    return lax.ppermute(value, axis, [(source, source + steps) for source in range(first, last)])


def window_sums(extended, length, halo_depth):
    options = []
    running = extended
    stride = 1
    for level_idx in range(4):
        running = running[stride:] + running[:-stride]
        stride = stride * 2
        offset = halo_depth - (stride - 1)
        options.append(running[offset : offset + length])
    return options


def pool_groups(pool_input, group_mix, group_scale):
    halo_depth = 15
    tok_rows = pool_input.shape[0]
    local_groups, group_width = (group_mix.shape[0], group_mix.shape[1])
    previous = shifted(pool_input[tok_rows - halo_depth :], "ep", 1)
    extended = jnp.concatenate([previous, pool_input], axis=0).astype(jnp.float32)
    options = window_sums(extended, tok_rows, halo_depth)
    position = lax.axis_index("ep") * tok_rows + lax.iota(jnp.int32, tok_rows)
    first_group = lax.axis_index("tp") * local_groups
    group_id = first_group + 0
    trailing = jnp.zeros((tok_rows, group_width), jnp.float32)
    for level_idx in range(4):
        trailing = trailing + jnp.where(group_id == level_idx, options[level_idx], 0.0)
    window_len = jnp.left_shift(jnp.int32(2), group_id)
    counted = jnp.minimum(position + 1, window_len).astype(jnp.float32)
    pooled = (trailing / counted[:, None] - extended[halo_depth:, 0:group_width]).astype(
        jnp.bfloat16
    )
    grouped = jnp.dot(pooled, group_mix[0], preferred_element_type=jnp.float32)
    pieces = (grouped * group_scale).astype(jnp.bfloat16)
    return pieces


def expert_block(received, gate_proj, up_proj, down_proj):
    local_experts = gate_proj.shape[0]
    sources = received.shape[0] // local_experts
    slot_grid = received.reshape(sources, local_experts, received.shape[1], received.shape[2])
    gate_part = jnp.einsum(
        "sjnd,jdf->sjnf", slot_grid, gate_proj, preferred_element_type=jnp.float32
    )
    up_part = jnp.einsum("sjnd,jdf->sjnf", slot_grid, up_proj, preferred_element_type=jnp.float32)
    active = (jax.nn.silu(gate_part) * up_part).astype(jnp.bfloat16)
    result = jnp.einsum(
        "sjnf,jfd->sjnd", active, down_proj, preferred_element_type=jnp.float32
    ).astype(jnp.bfloat16)
    return result.reshape(received.shape)


def route_experts(moe_input, norm_gain, expert_ids, expert_scores, gate_proj, up_proj, down_proj):
    tok_rows, model_width = moe_input.shape
    top_count = expert_ids.shape[1]
    experts_all = lax.axis_size("ep") * lax.axis_size("tp") * gate_proj.shape[0]
    capacity = 2 * tok_rows * top_count // experts_all
    values = moe_input.astype(jnp.float32)
    normed = (
        values * lax.rsqrt(jnp.mean(values * values, axis=1, keepdims=True) + epsilon) * norm_gain
    ).astype(jnp.bfloat16)
    flat_ids = expert_ids.reshape(-1)
    onehot = (flat_ids[:, None] == lax.iota(jnp.int32, experts_all)[None, :]).astype(jnp.int32)
    earlier = jnp.cumsum(onehot, axis=0) - onehot
    slot_in = jnp.sum(earlier * onehot, axis=1)
    target = flat_ids * capacity + slot_in
    token_of = lax.iota(jnp.int32, tok_rows * top_count) // top_count
    slot_token = jnp.full((experts_all * capacity,), tok_rows, jnp.int32).at[target].set(token_of)
    padded = jnp.concatenate([normed, jnp.zeros((1, model_width), jnp.bfloat16)], axis=0)
    outbound = padded[slot_token].reshape(experts_all, capacity, model_width)
    returned = lax.all_to_all(
        expert_block(
            lax.all_to_all(outbound, ("ep", "tp"), split_axis=0, concat_axis=0, tiled=True),
            gate_proj,
            up_proj,
            down_proj,
        ),
        ("ep", "tp"),
        split_axis=0,
        concat_axis=0,
        tiled=True,
    )
    picked = returned.reshape(experts_all * capacity, model_width)[target]
    picked = picked.astype(jnp.float32).reshape(tok_rows, top_count, model_width)
    weights = expert_scores / jnp.sum(expert_scores, axis=1, keepdims=True)
    return jnp.sum(picked * weights[:, :, None], axis=1).astype(jnp.bfloat16)


def body(
    pool_input,
    group_mix,
    group_scale,
    out_proj,
    moe_input,
    norm_gain,
    expert_ids,
    expert_scores,
    gate_proj,
    up_proj,
    down_proj,
):
    hidden = pool_groups(pool_input, group_mix, group_scale)
    gathered = lax.all_to_all(hidden, "tp", split_axis=0, concat_axis=1, tiled=True)
    mixed_tokens = jnp.dot(gathered, out_proj, preferred_element_type=jnp.float32).astype(
        jnp.bfloat16
    )
    mixed_experts = route_experts(
        moe_input, norm_gain, expert_ids, expert_scores, gate_proj, up_proj, down_proj
    )
    return (mixed_tokens, mixed_experts)


def solution(mesh):
    placed = (
        P("ep", "tp"),
        P("tp", None, None),
        P("tp"),
        P(),
        P(("ep", "tp"), None),
        P(),
        P(("ep", "tp"), None),
        P(("ep", "tp"), None),
        P(("ep", "tp"), None, None),
        P(("ep", "tp"), None, None),
        P(("ep", "tp"), None, None),
    )
    return jax.shard_map(
        body,
        mesh=mesh,
        in_specs=placed,
        out_specs=(P(("ep", "tp"), None), P(("ep", "tp"), None)),
        check_vma=False,
    )
```

profile of v0, /device:TPU:11, one launch (start us, length us, event | category | flops | bytes accessed | tf_op | source)
XLA Modules:
  0.0 157.8 jit_solution(2295768085454617710)
XLA Ops:
  0.6 0.8 copy.16
  1.6 0.1 eq.41
  1.8 0.7 broadcast_multiply_fusion
  2.5 0.6 reduce-window.6
  3.1 0.2 slice_reduce_fusion
  3.4 0.1 mul.74
  3.7 1.4 scatter_custom_fusion
  5.1 1.2 fusion.26
  6.3 1.2 fusion.28
  7.6 3.3 %gather_fusion = bf16[512,2048]{1,0:T(8,128)(2,1)} fusion(bf16[129,2048]{1,0:T(8,128)(2,1)S(1)} %concatenate.7, s32[1024]{0:T(1024)S(1)} %pad_clamp_fusion.1), kind=kCustom, calls=%fused_computation | custom fusion | bytes 4196352 | tf_op jit(solution)/shard_map/gather | solution.py:82
  11.0 6.3 %all-to-all-start.1 = ((bf16[32,16,2048]{2,1,0:T(8,128)(2,1)}), bf16[32,16,2048]{2,1,0:T(8,128)(2,1)S(1)}, u32[]{:S(2)}, u32[]{:S(2)}) async-start(bf16[32,16,2048]{2,1,0:T(8,128)(2,1)} %bitcast.7), calls=%async_computation.1 | async-start | bytes 4194304 | tf_op jit(solution)/shard_map/all_to_all | solution.py:85
  17.3 0.7 slice.43
  18.0 3.1 %collective-permute-start = (bf16[15,512]{1,0:T(8,128)(2,1)S(1)}, bf16[15,512]{1,0:T(8,128)(2,1)S(1)}, u32[]{:S(2)}, u32[]{:S(2)}) collective-permute-start(bf16[15,512]{1,0:T(8,128)(2,1)S(1)} %slice.43), channel_id=1, source_target_pairs={{0,4},{4,8},{8,12},{12,16},{16,20},{20,24},{24,28},{1,5},{5,9},{9,... | collective-permute-start | bytes 46088 | tf_op jit(solution)/shard_map/ppermute | solution.py:12
  21.1 32.2 %collective-permute-done = bf16[15,512]{1,0:T(8,128)(2,1)S(1)} collective-permute-done((bf16[15,512]{1,0:T(8,128)(2,1)S(1)}, bf16[15,512]{1,0:T(8,128)(2,1)S(1)}, u32[]{:S(2)}, u32[]{:S(2)}) %collective-permute-start) | collective-permute-done | bytes 15392 | tf_op jit(solution)/shard_map/ppermute | solution.py:12
  53.4 1.9 %maximum_convert_fusion = f32[1551,512]{1,0:T(8,128)S(1)} fusion(bf16[1536,512]{1,0:T(8,128)(2,1)} %param.11, bf16[15,512]{1,0:T(8,128)(2,1)S(1)} %collective-permute-done), kind=kLoop, calls=%fused_computation.34 | loop fusion | flops 3176448 | bytes 4764672 | tf_op jit(solution)/shard_map/convert_element_type | solution.py:32
  55.2 0.4 slice_add_fusion.1
  55.7 0.4 slice_add_fusion
  56.1 0.4 slice_add_fusion.2
  56.5 0.2 copy-done.2
  56.8 3.2 %fusion.15 = bf16[1536,512]{1,0:T(8,128)(2,1)} fusion(f32[512]{0:T(512)S(1)} %copy-done.2, f32[1551,512]{1,0:T(8,128)S(1)} %maximum_convert_fusion, f32[1544,512]{1,0:T(8,128)S(1)} %slice_add_fusion.2, f32[1548,512]{1,0:T(8,128)S(1)} %slice_add_fusion, f32[1550,512]{1,0:T(8,128)S(1)} %slice_add_fusion.1, f32[1536]{0:T(1024)S(1)} %minimum_convert_fusion, ...), kind=kOutput, calls=%fused_computation.24 | convolution fusion | flops 815529984 | bytes 17836036 | tf_op jit(solution)/shard_map/dot_general | solution.py:45
  60.0 2.6 %copy.14 = bf16[4,384,512]{1,2,0:T(8,128)(2,1)} copy(bf16[4,384,512]{2,1,0:T(8,128)(2,1)} %bitcast.92) | data formatting | bytes 3145728 | tf_op jit(solution)/shard_map/all_to_all | solution.py:115
  62.6 2.0 %all-to-all-done.1 = bf16[32,16,2048]{2,1,0:T(8,128)(2,1)S(1)} async-done(((bf16[32,16,2048]{2,1,0:T(8,128)(2,1)}), bf16[32,16,2048]{2,1,0:T(8,128)(2,1)S(1)}, u32[]{:S(2)}, u32[]{:S(2)}) %all-to-all-start.1) | async-done | bytes 2097184 | tf_op jit(solution)/shard_map/all_to_all | solution.py:85
  64.6 4.3 %all-to-all-start = ((bf16[4,384,512]{1,2,0:T(8,128)(2,1)}), bf16[4,384,512]{1,2,0:T(8,128)(2,1)}, u32[]{:S(2)}, u32[]{:S(2)}) async-start(bf16[4,384,512]{1,2,0:T(8,128)(2,1)} %copy.14), calls=%async_computation | async-start | bytes 3145728 | tf_op jit(solution)/shard_map/all_to_all | solution.py:115
  69.0 5.8 %fusion.4 = f32[32,16,1024]{2,1,0:T(8,128)} fusion(bf16[32,16,2048]{2,1,0:T(8,128)(2,1)S(1)} %all-to-all-done.1, bf16[1,2048,1024]{2,1,0:T(8,128)(2,1)} %param.19), kind=kOutput, calls=%fused_computation.7 | convolution fusion | flops 2147483648 | bytes 8388608 | tf_op jit(solution)/shard_map/sjnd,jdf->sjnf/dot_general | solution.py:54
  74.8 10.0 %fusion.12 = bf16[32,16,2048]{2,1,0:T(8,128)(2,1)} fusion(bf16[1,1024,2048]{2,1,0:T(8,128)(2,1)} %param.21, bf16[32,16,2048]{2,1,0:T(8,128)(2,1)S(1)} %all-to-all-done.1, bf16[1,2048,1024]{2,1,0:T(8,128)(2,1)} %param.20, f32[32,16,1024]{2,1,0:T(8,128)} %fusion.4), kind=kOutput, calls=%fused_computation.23 | convolution fusion | flops 4299161600 | bytes 14680064 | tf_op jit(solution)/shard_map/sjnf,jfd->sjnd/dot_general | solution.py:59
  84.8 2.6 %all-to-all-done = bf16[4,384,512]{1,2,0:T(8,128)(2,1)} async-done(((bf16[4,384,512]{1,2,0:T(8,128)(2,1)}), bf16[4,384,512]{1,2,0:T(8,128)(2,1)}, u32[]{:S(2)}, u32[]{:S(2)}) %all-to-all-start) | async-done | bytes 1572896 | tf_op jit(solution)/shard_map/all_to_all | solution.py:115
  87.3 14.5 %all-to-all-start.2 = ((bf16[32,16,2048]{2,1,0:T(8,128)(2,1)}), bf16[32,16,2048]{2,1,0:T(8,128)(2,1)S(1)}, u32[]{:S(2)}, u32[]{:S(2)}) async-start(bf16[32,16,2048]{2,1,0:T(8,128)(2,1)} %fusion.12), calls=%async_computation.2 | async-start | bytes 4194304 | tf_op jit(solution)/shard_map/all_to_all | solution.py:83
  102.0 8.5 %convolution_convert_fusion = bf16[384,2048]{1,0:T(8,128)(2,1)} fusion(bf16[384,2048]{0,1:T(8,128)(2,1)} %bitcast.3, bf16[2048,2048]{1,0:T(8,128)(2,1)} %param.14), kind=kOutput, calls=%fused_computation.25 | convolution fusion | flops 3222011904 | bytes 11534336 | tf_op jit(solution)/shard_map/dot_general | solution.py:116
  110.5 38.7 %all-to-all-done.2 = bf16[32,16,2048]{2,1,0:T(8,128)(2,1)S(1)} async-done(((bf16[32,16,2048]{2,1,0:T(8,128)(2,1)}), bf16[32,16,2048]{2,1,0:T(8,128)(2,1)S(1)}, u32[]{:S(2)}, u32[]{:S(2)}) %all-to-all-start.2) | async-done | bytes 2097184 | tf_op jit(solution)/shard_map/all_to_all | solution.py:83
  149.2 2.3 %gather_fusion.1 = bf16[256,2048]{1,0:T(8,128)(2,1)} fusion(bf16[512,2048]{1,0:T(8,128)(2,1)S(1)} %bitcast.91, s32[1024]{0:T(1024)S(1)} %pad_clamp_fusion), kind=kCustom, calls=%fused_computation.1 | custom fusion | bytes 2098176 | tf_op jit(solution)/shard_map/gather | solution.py:95
  151.5 2.4 %reshape.111 = f32[128,2,2048]{2,1,0:T(2,128)S(1)} reshape(bf16[256,2048]{1,0:T(8,128)(2,1)} %gather_fusion.1) | data formatting | bytes 3145728 | tf_op jit(solution)/shard_map/convert_element_type | solution.py:96
  153.9 3.9 %multiply_reduce_fusion = bf16[128,2048]{1,0:T(8,128)(2,1)} fusion(f32[128,2,2048]{2,1,0:T(2,128)S(1)} %reshape.111, f32[128,2]{1,0:T(8,128)S(1)} %copy.19), kind=kLoop, calls=%fused_computation.33 | loop fusion | flops 786432 | bytes 2622464 | tf_op jit(solution)/shard_map/reduce_sum | solution.py:98
  (22 shorter events, 0.6 us)
Async XLA Ops:
  0.6 55.9 %copy-start = (bf16[1,512,512]{2,1,0:T(8,128)(2,1)S(1)}, bf16[1,512,512]{2,1,0:T(8,128)(2,1)}, u32[]{:S(2)}) copy-start(bf16[1,512,512]{2,1,0:T(8,128)(2,1)} %param.12) | copy-start | bytes 1572868
  11.0 53.7 %all-to-all-start.1 = ((bf16[32,16,2048]{2,1,0:T(8,128)(2,1)}), bf16[32,16,2048]{2,1,0:T(8,128)(2,1)S(1)}, u32[]{:S(2)}, u32[]{:S(2)}) async-start(bf16[32,16,2048]{2,1,0:T(8,128)(2,1)} %bitcast.7), calls=%async_computation.1 | async-start | bytes 4194304 | tf_op jit(solution)/shard_map/all_to_all | solution.py:85
  18.0 35.4 %collective-permute-start = (bf16[15,512]{1,0:T(8,128)(2,1)S(1)}, bf16[15,512]{1,0:T(8,128)(2,1)S(1)}, u32[]{:S(2)}, u32[]{:S(2)}) collective-permute-start(bf16[15,512]{1,0:T(8,128)(2,1)S(1)} %slice.43), channel_id=1, source_target_pairs={{0,4},{4,8},{8,12},{12,16},{16,20},{20,24},{24,28},{1,5},{5,9},{9,... | collective-permute-start | bytes 46088 | tf_op jit(solution)/shard_map/ppermute | solution.py:12
  56.1 0.7 copy-start.2
  64.6 22.7 %all-to-all-start = ((bf16[4,384,512]{1,2,0:T(8,128)(2,1)}), bf16[4,384,512]{1,2,0:T(8,128)(2,1)}, u32[]{:S(2)}, u32[]{:S(2)}) async-start(bf16[4,384,512]{1,2,0:T(8,128)(2,1)} %copy.14), calls=%async_computation | async-start | bytes 3145728 | tf_op jit(solution)/shard_map/all_to_all | solution.py:115
  84.8 17.1 %copy-start.1 = (f32[128,2]{0,1:T(2,128)S(1)}, f32[128,2]{0,1:T(2,128)}, u32[]{:S(2)}) copy-start(f32[128,2]{0,1:T(2,128)} %param.18) | copy-start | bytes 3076
  87.3 61.9 %all-to-all-start.2 = ((bf16[32,16,2048]{2,1,0:T(8,128)(2,1)}), bf16[32,16,2048]{2,1,0:T(8,128)(2,1)S(1)}, u32[]{:S(2)}, u32[]{:S(2)}) async-start(bf16[32,16,2048]{2,1,0:T(8,128)(2,1)} %fusion.12), calls=%async_computation.2 | async-start | bytes 4194304 | tf_op jit(solution)/shard_map/all_to_all | solution.py:83
where the time goes:
time: 161 us; the launch traced here: 158 us
  waiting for transfers between devices  75.6 us (47%)
  starting transfers between devices  28.2 us (18%)
  matrix products  27.5 us (17%)
  local copies, waits for them, and re-layouts  14.8 us (9%)
  other arithmetic  11 us (7%)
    all_to_all x1, waiting for transfers between devices, route_experts(): lax.all_to_all(expert_block(lax.all_to_all(outbound, ('ep', 'tp'), split_...  38.7 us
    ppermute x1, waiting for transfers between devices, shifted(): lax.ppermute(value, axis, [(source, source + steps) for source in range(f...  32.2 us
    all_to_all x1, starting transfers between devices, route_experts(): lax.all_to_all(expert_block(lax.all_to_all(outbound, ('ep', 'tp'), split_...  14.5 us
    dot_general x1, matrix products, expert_block(): jnp.einsum('sjnf,jfd->sjnd', active, down_proj, preferred_element_type=jn...  9.96 us
    dot_general x1, matrix products, body(): jnp.dot(gathered, out_proj, preferred_element_type=jnp.float32)  8.49 us
    all_to_all x1, starting transfers between devices, route_experts(): lax.all_to_all(outbound, ('ep', 'tp'), split_axis=0, concat_axis=0, tiled...  6.3 us
    dot_general x1, matrix products, expert_block(): jnp.einsum('sjnd,jdf->sjnf', slot_grid, gate_proj, preferred_element_type...  5.81 us
    all_to_all x1, starting transfers between devices, body(): lax.all_to_all(hidden, 'tp', split_axis=0, concat_axis=1, tiled=True)  4.34 us
  transfers between devices with their start and end apart: 4, of which 4 were waited for; matrix products, arithmetic and copies ran while one was open for 22% of the time, Pallas kernels for 0%

commit v1 on v0

--- a/solution.py
+++ b/solution.py
@@ -49,17 +49,32 @@
 
 def expert_block(received, gate_proj, up_proj, down_proj):
     local_experts = gate_proj.shape[0]
-    sources = received.shape[0] // local_experts
-    slot_grid = received.reshape(sources, local_experts, received.shape[1], received.shape[2])
-    gate_part = jnp.einsum(
-        "sjnd,jdf->sjnf", slot_grid, gate_proj, preferred_element_type=jnp.float32
-    )
-    up_part = jnp.einsum("sjnd,jdf->sjnf", slot_grid, up_proj, preferred_element_type=jnp.float32)
-    active = (jax.nn.silu(gate_part) * up_part).astype(jnp.bfloat16)
-    result = jnp.einsum(
-        "sjnf,jfd->sjnd", active, down_proj, preferred_element_type=jnp.float32
-    ).astype(jnp.bfloat16)
-    return result.reshape(received.shape)
+    sources, rows, width = received.shape
+    slot_grid = received.reshape(sources // local_experts, local_experts, rows, width)
+    results = []
+    for j in range(local_experts):
+        slots = slot_grid[:, j].reshape(-1, width)
+        gate_part = jnp.dot(slots, gate_proj[j], preferred_element_type=jnp.float32)
+        up_part = jnp.dot(slots, up_proj[j], preferred_element_type=jnp.float32)
+        active = (jax.nn.silu(gate_part) * up_part).astype(jnp.bfloat16)
+        result = jnp.dot(active, down_proj[j], preferred_element_type=jnp.float32)
+        results.append(result.astype(jnp.bfloat16).reshape(-1, 1, rows, width))
+    return jnp.concatenate(results, axis=1).reshape(received.shape)
+
+
+def slot_targets(expert_ids, experts_all, capacity):
+    tok_rows, top_count = expert_ids.shape
+    experts = lax.iota(jnp.int32, experts_all)[None, :]
+    chosen = [expert_ids[:, k : k + 1] == experts for k in range(top_count)]
+    named = sum(pick.astype(jnp.bfloat16) for pick in chosen)
+    rows = lax.iota(jnp.int32, tok_rows)
+    before = (rows[:, None] > rows[None, :]).astype(jnp.bfloat16)
+    earlier = jnp.dot(before, named, preferred_element_type=jnp.float32)
+    targets = []
+    for k in range(top_count):
+        slot = jnp.sum(jnp.where(chosen[k], earlier, 0.0), axis=1).astype(jnp.int32)
+        targets.append(expert_ids[:, k] * capacity + slot)
+    return targets
 
 
 def route_experts(moe_input, norm_gain, expert_ids, expert_scores, gate_proj, up_proj, down_proj):
@@ -71,15 +86,11 @@
     normed = (
         values * lax.rsqrt(jnp.mean(values * values, axis=1, keepdims=True) + epsilon) * norm_gain
     ).astype(jnp.bfloat16)
-    flat_ids = expert_ids.reshape(-1)
-    onehot = (flat_ids[:, None] == lax.iota(jnp.int32, experts_all)[None, :]).astype(jnp.int32)
-    earlier = jnp.cumsum(onehot, axis=0) - onehot
-    slot_in = jnp.sum(earlier * onehot, axis=1)
-    target = flat_ids * capacity + slot_in
-    token_of = lax.iota(jnp.int32, tok_rows * top_count) // top_count
-    slot_token = jnp.full((experts_all * capacity,), tok_rows, jnp.int32).at[target].set(token_of)
-    padded = jnp.concatenate([normed, jnp.zeros((1, model_width), jnp.bfloat16)], axis=0)
-    outbound = padded[slot_token].reshape(experts_all, capacity, model_width)
+    targets = slot_targets(expert_ids, experts_all, capacity)
+    slots = lax.iota(jnp.int32, experts_all * capacity)
+    fill = sum((slots[:, None] == t[None, :]).astype(jnp.bfloat16) for t in targets)
+    outbound = jnp.dot(fill, normed, preferred_element_type=jnp.float32).astype(jnp.bfloat16)
+    outbound = outbound.reshape(experts_all, capacity, model_width)
     returned = lax.all_to_all(
         expert_block(
             lax.all_to_all(outbound, ("ep", "tp"), split_axis=0, concat_axis=0, tiled=True),
@@ -91,11 +102,31 @@
         split_axis=0,
         concat_axis=0,
         tiled=True,
+    ).reshape(experts_all * capacity, model_width)
+    weights = expert_scores / jnp.sum(expert_scores, axis=1, keepdims=True)
+    spread = sum(
+        jnp.where(slots[None, :] == targets[k][:, None], weights[:, k : k + 1], 0.0)
+        for k in range(top_count)
     )
-    picked = returned.reshape(experts_all * capacity, model_width)[target]
-    picked = picked.astype(jnp.float32).reshape(tok_rows, top_count, model_width)
-    weights = expert_scores / jnp.sum(expert_scores, axis=1, keepdims=True)
-    return jnp.sum(picked * weights[:, :, None], axis=1).astype(jnp.bfloat16)
+    coarse = lax.reduce_precision(spread, 8, 7)
+    fine = (spread - coarse).astype(jnp.bfloat16)
+    mixed = jnp.dot(coarse.astype(jnp.bfloat16), returned, preferred_element_type=jnp.float32)
+    mixed = mixed + jnp.dot(fine, returned, preferred_element_type=jnp.float32)
+    return mixed.astype(jnp.bfloat16)
+
+
+def exchange_groups(hidden):
+    count = lax.axis_size("tp")
+    me = lax.axis_index("tp")
+    rows, width = hidden.shape[0] // count, hidden.shape[1]
+    gathered = jnp.zeros((rows, count * width), hidden.dtype)
+    for step in range(count):
+        dest, source = lax.rem(me + step, count), lax.rem(me + count - step, count)
+        block = lax.dynamic_slice_in_dim(hidden, dest * rows, rows, 0)
+        if step:
+            block = lax.ppermute(block, "tp", [(i, (i + step) % count) for i in range(count)])
+        gathered = lax.dynamic_update_slice(gathered, block, (0, source * width))
+    return gathered
 
 
 def body(
@@ -112,7 +143,7 @@
     down_proj,
 ):
     hidden = pool_groups(pool_input, group_mix, group_scale)
-    gathered = lax.all_to_all(hidden, "tp", split_axis=0, concat_axis=1, tiled=True)
+    gathered = exchange_groups(hidden)
     mixed_tokens = jnp.dot(gathered, out_proj, preferred_element_type=jnp.float32).astype(
         jnp.bfloat16
     )

time: 161 us -> 142 us (0.88)
  waiting for transfers between devices: 75.6 us -> 63.4 us
  starting transfers between devices: 28.2 us -> 21.6 us
  matrix products: 27.5 us -> 31.8 us
  local copies, waits for them, and re-layouts: 14.8 us -> 12.2 us
    all_to_all x1, waiting for transfers between devices: 38.7 us -> 0.01 us  [route_experts(): lax.all_to_all(expert_block(lax.all_to_all(outbound, ('ep', 'tp'), split_...]
    ppermute x0 -> x3, waiting for transfers between devices: none -> 25.6 us  [exchange_groups(): lax.ppermute(block, 'tp', [(i, (i + step) % count) for i in range(count)])]
    gather x2 -> x0, local copies, waits for them, and re-layouts: 5.69 us -> none  [the longest x1 3.35 us: route_experts(): outbound = padded[slot_token].reshape(experts_all, capacity, model_width)]
    dot_general x2 -> x6, matrix products: 15.8 us -> 21 us  [the longest x1 9.94 us: expert_block(): result = jnp.dot(active, down_proj[j], preferred_element_type=jnp.float32)]
    add x3, other arithmetic: 1.25 us -> 6.16 us  [window_sums(): running = running[stride:] + running[:-stride]]
    dynamic_update_slice x0 -> x3, local copies, waits for them, and re-layouts: none -> 4.46 us  [exchange_groups(): gathered = lax.dynamic_update_slice(gathered, block, (0, source * width))]
    all_to_all x1 -> x0, starting transfers between devices: 4.34 us -> none  [body(): lax.all_to_all(hidden, 'tp', split_axis=0, concat_axis=1, tiled=True)]
    unnamed x7 -> x16, local copies, waits for them, and re-layouts: 1.1 us -> 5.2 us
  transfers between devices with their start and end apart: 4 -> 6, of which waited for: 4 -> 4; matrix products, arithmetic and copies ran while one was open for 22% -> 18% of each run, Pallas kernels for 0% -> 0%
where the time goes in v1:
time: 142 us; the launch traced here: 140 us
  waiting for transfers between devices  63.4 us (45%)
  matrix products  31.8 us (22%)
  starting transfers between devices  21.6 us (15%)
  local copies, waits for them, and re-layouts  12.2 us (9%)
  other arithmetic  10.1 us (7%)
    ppermute x1, waiting for transfers between devices, shifted(): lax.ppermute(value, axis, [(source, source + steps) for source in range(f...  32.1 us
    ppermute x3, waiting for transfers between devices, exchange_groups(): lax.ppermute(block, 'tp', [(i, (i + step) % count) for i in range(count)])  25.6 us
    all_to_all x1, starting transfers between devices, route_experts(): lax.all_to_all(expert_block(lax.all_to_all(outbound, ('ep', 'tp'), split_...  10.5 us
    dot_general x1, matrix products, expert_block(): result = jnp.dot(active, down_proj[j], preferred_element_type=jnp.float32)  9.94 us
    dot_general x1, matrix products, body(): jnp.dot(gathered, out_proj, preferred_element_type=jnp.float32)  8.42 us
    all_to_all x1, starting transfers between devices, route_experts(): lax.all_to_all(outbound, ('ep', 'tp'), split_axis=0, concat_axis=0, tiled...  6.3 us
    add x3, other arithmetic, window_sums(): running = running[stride:] + running[:-stride]  6.16 us
    dot_general x1, matrix products, expert_block(): gate_part = jnp.dot(slots, gate_proj[j], preferred_element_type=jnp.float32)  5.89 us
  transfers between devices with their start and end apart: 6, of which 4 were waited for; matrix products, arithmetic and copies ran while one was open for 18% of the time, Pallas kernels for 0%

profile of v1, /device:TPU:11, one launch (start us, length us, event | category | flops | bytes accessed | tf_op | source)
XLA Modules:
  0.0 140.0 jit_solution(18084995706768360777)
XLA Ops:
  0.6 1.3 fusion.20
  1.9 0.8 slice_bitcast_fusion.3
  2.9 0.8 multiply_add_fusion.1
  3.6 3.2 %convolution_convert_fusion = bf16[512,2048]{1,0:T(8,128)(2,1)} fusion(bf16[128,2048]{1,0:T(8,128)(2,1)} %param.15, f32[2048]{0:T(1024)} %param.16, f32[128]{0:T(128)S(1)} %add_rsqrt_fusion, s32[128]{0:T(128)S(1)} %get-tuple-element.13, s32[128]{0:T(128)S(1)} %get-tuple-element.12), kind=kOutput, calls=%fused_computation.21 | convolution fusion | flops 271056896 | bytes 2631168 | tf_op jit(solution)/shard_map/dot_general | solution.py:92
  6.9 6.3 %all-to-all-start = ((bf16[32,16,2048]{2,1,0:T(8,128)(2,1)}), bf16[32,16,2048]{2,1,0:T(8,128)(2,1)S(1)}, u32[]{:S(2)}, u32[]{:S(2)}) async-start(bf16[32,16,2048]{2,1,0:T(8,128)(2,1)} %bitcast.9), calls=%async_computation | async-start | bytes 4194304 | tf_op jit(solution)/shard_map/all_to_all | solution.py:96
  13.2 0.7 slice.51
  13.9 3.1 %collective-permute-start = (bf16[15,512]{1,0:T(8,128)(2,1)S(1)}, bf16[15,512]{1,0:T(8,128)(2,1)S(1)}, u32[]{:S(2)}, u32[]{:S(2)}) collective-permute-start(bf16[15,512]{1,0:T(8,128)(2,1)S(1)} %slice.51), channel_id=1, source_target_pairs={{0,4},{4,8},{8,12},{12,16},{16,20},{20,24},{24,28},{1,5},{5,9},{9,... | collective-permute-start | bytes 46088 | tf_op jit(solution)/shard_map/ppermute | solution.py:12
  17.1 32.1 %collective-permute-done = bf16[15,512]{1,0:T(8,128)(2,1)S(1)} collective-permute-done((bf16[15,512]{1,0:T(8,128)(2,1)S(1)}, bf16[15,512]{1,0:T(8,128)(2,1)S(1)}, u32[]{:S(2)}, u32[]{:S(2)}) %collective-permute-start) | collective-permute-done | bytes 15392 | tf_op jit(solution)/shard_map/ppermute | solution.py:12
  49.3 1.9 %maximum_convert_fusion = f32[1551,512]{1,0:T(8,128)S(1)} fusion(bf16[1536,512]{1,0:T(8,128)(2,1)} %param.11, bf16[15,512]{1,0:T(8,128)(2,1)S(1)} %collective-permute-done), kind=kLoop, calls=%fused_computation.27 | loop fusion | flops 3176448 | bytes 4764672 | tf_op jit(solution)/shard_map/convert_element_type | solution.py:32
  51.1 1.6 %copy-done.1 = f32[1551,512]{1,0:T(8,128)} copy-done((f32[1551,512]{1,0:T(8,128)}, f32[1551,512]{1,0:T(8,128)S(1)}, u32[]{:S(2)}) %copy-start.1) | copy-done | bytes 3176472
  52.8 2.1 %slice_add_fusion.1 = f32[1550,512]{1,0:T(8,128)} fusion(f32[1551,512]{1,0:T(8,128)S(1)} %maximum_convert_fusion), kind=kLoop, calls=%fused_computation.8 | loop fusion | flops 793600 | bytes 9523200 | tf_op jit(solution)/shard_map/add | solution.py:20
  54.8 5.7 %all-to-all-done = bf16[32,16,2048]{2,1,0:T(8,128)(2,1)S(1)} async-done(((bf16[32,16,2048]{2,1,0:T(8,128)(2,1)}), bf16[32,16,2048]{2,1,0:T(8,128)(2,1)S(1)}, u32[]{:S(2)}, u32[]{:S(2)}) %all-to-all-start) | async-done | bytes 2097184 | tf_op jit(solution)/shard_map/all_to_all | solution.py:96
  60.5 5.9 %fusion.4 = f32[512,1024]{1,0:T(8,128)} fusion(bf16[512,2048]{1,0:T(8,128)(2,1)S(1)} %bitcast.54, bf16[1,2048,1024]{2,1,0:T(8,128)(2,1)} %param.19), kind=kOutput, calls=%fused_computation.4 | convolution fusion | flops 2147483648 | bytes 8388608 | tf_op jit(solution)/shard_map/dot_general | solution.py:57
  66.4 9.9 %fusion.12 = bf16[512,2048]{1,0:T(8,128)(2,1)} fusion(bf16[1,1024,2048]{2,1,0:T(8,128)(2,1)} %param.21, f32[512,1024]{1,0:T(8,128)} %fusion.4, bf16[512,2048]{1,0:T(8,128)(2,1)S(1)} %bitcast.55, bf16[1,2048,1024]{2,1,0:T(8,128)(2,1)} %param.20), kind=kOutput, calls=%fused_computation.20 | convolution fusion | flops 4299161600 | bytes 14680064 | tf_op jit(solution)/shard_map/dot_general | solution.py:60
  76.4 10.5 %all-to-all-start.1 = ((bf16[32,16,2048]{2,1,0:T(8,128)(2,1)}), bf16[32,16,2048]{2,1,0:T(8,128)(2,1)S(1)}, u32[]{:S(2)}, u32[]{:S(2)}) async-start(bf16[32,16,2048]{2,1,0:T(8,128)(2,1)} %bitcast.56), calls=%async_computation.1 | async-start | bytes 4194304 | tf_op jit(solution)/shard_map/all_to_all | solution.py:94
  86.9 3.7 %slice_add_fusion = f32[1548,512]{1,0:T(8,128)S(1)} fusion(f32[1550,512]{1,0:T(8,128)} %slice_add_fusion.1), kind=kLoop, calls=%fused_computation.7 | loop fusion | flops 792576 | bytes 9510912 | tf_op jit(solution)/shard_map/add | solution.py:20
  90.6 0.4 slice_add_fusion.2
  91.0 1.4 %copy-done.2 = f32[1551,512]{1,0:T(8,128)S(1)} copy-done((f32[1551,512]{1,0:T(8,128)S(1)}, f32[1551,512]{1,0:T(8,128)}, u32[]{:S(2)}) %copy-start.2) | copy-done | bytes 3176472
  92.4 1.0 copy-done.3
  93.4 2.3 %fusion.15 = bf16[1536,512]{1,0:T(8,128)(2,1)S(1)} fusion(f32[512]{0:T(512)S(1)} %copy-done.7, f32[1551,512]{1,0:T(8,128)S(1)} %copy-done.2, f32[1544,512]{1,0:T(8,128)S(1)} %slice_add_fusion.2, f32[1548,512]{1,0:T(8,128)S(1)} %slice_add_fusion, f32[1550,512]{1,0:T(8,128)S(1)} %copy-done.3, f32[1536]{0:T(1024)S(1)} %minimum_convert_fusion, pred[]{:T(512)S(6)} %eq.101, ...), kind=kOutput, calls=%fused_computation.22 | convolution fusion | flops 815529984 | bytes 17836036 | tf_op jit(solution)/shard_map/dot_general | solution.py:45
  95.9 0.9 constant_dynamic-slice_fusion
  96.8 1.1 copy-done.4
  98.0 0.6 collective-permute-start.1
  98.5 1.2 collective-permute-start.2
  99.7 14.5 %collective-permute-done.1 = bf16[384,512]{1,0:T(8,128)(2,1)} collective-permute-done((bf16[384,512]{1,0:T(8,128)(2,1)}, bf16[384,512]{1,0:T(8,128)(2,1)}, u32[]{:S(2)}, u32[]{:S(2)}) %collective-permute-start.1) | collective-permute-done | bytes 393248 | tf_op jit(solution)/shard_map/ppermute | solution.py:127
  114.2 1.8 %constant_dynamic-update-slice_fusion.1 = bf16[384,2048]{1,0:T(8,128)(2,1)} fusion(bf16[384,2048]{1,0:T(8,128)(2,1)} %copy-done.4, bf16[384,512]{1,0:T(8,128)(2,1)} %collective-permute-done.1, s32[]{:T(128)S(6)} %select_n.75), kind=kLoop, calls=%fused_computation.76 | loop fusion | bytes 786436 | tf_op jit(solution)/shard_map/dynamic_update_slice | solution.py:128
  116.0 11.1 %collective-permute-done.2 = bf16[384,512]{1,0:T(8,128)(2,1)} collective-permute-done((bf16[384,512]{1,0:T(8,128)(2,1)S(1)}, bf16[384,512]{1,0:T(8,128)(2,1)}, u32[]{:S(2)}, u32[]{:S(2)}) %collective-permute-start.2) | collective-permute-done | bytes 393248 | tf_op jit(solution)/shard_map/ppermute | solution.py:127
  127.1 1.8 %constant_dynamic-update-slice_fusion = bf16[384,2048]{1,0:T(8,128)(2,1)} fusion(bf16[384,2048]{1,0:T(8,128)(2,1)} %constant_dynamic-update-slice_fusion.1, bf16[384,512]{1,0:T(8,128)(2,1)} %collective-permute-done.2, s32[]{:T(128)S(6)} %select_n.77), kind=kLoop, calls=%fused_computation.74 | loop fusion | bytes 786436 | tf_op jit(solution)/shard_map/dynamic_update_slice | solution.py:128
  129.0 0.8 constant_dynamic-update-slice_fusion.2
  129.8 8.4 %convolution_convert_fusion.1 = bf16[384,2048]{1,0:T(8,128)(2,1)} fusion(bf16[384,2048]{1,0:T(8,128)(2,1)} %constant_dynamic-update-slice_fusion.2, bf16[2048,2048]{1,0:T(8,128)(2,1)} %param.14), kind=kOutput, calls=%fused_computation.23 | convolution fusion | flops 3222011904 | bytes 11534336 | tf_op jit(solution)/shard_map/dot_general | solution.py:147
  138.2 0.5 fusion.33
  138.7 1.3 fusion.16
  (23 shorter events, 0.4 us)
Async XLA Ops:
  0.6 90.4 %copy-start = (bf16[1,512,512]{2,1,0:T(8,128)(2,1)S(1)}, bf16[1,512,512]{2,1,0:T(8,128)(2,1)}, u32[]{:S(2)}) copy-start(bf16[1,512,512]{2,1,0:T(8,128)(2,1)} %param.12) | copy-start | bytes 1572868
  3.6 13.3 %copy-start.5 = (s32[128,2]{0,1:T(2,128)S(1)}, s32[128,2]{0,1:T(2,128)}, u32[]{:S(2)}) copy-start(s32[128,2]{0,1:T(2,128)} %param.17) | copy-start | bytes 3076
  3.6 13.4 %copy-start.6 = (f32[128,2]{0,1:T(2,128)S(1)}, f32[128,2]{0,1:T(2,128)}, u32[]{:S(2)}) copy-start(f32[128,2]{0,1:T(2,128)} %param.18) | copy-start | bytes 3076
  6.9 53.7 %all-to-all-start = ((bf16[32,16,2048]{2,1,0:T(8,128)(2,1)}), bf16[32,16,2048]{2,1,0:T(8,128)(2,1)S(1)}, u32[]{:S(2)}, u32[]{:S(2)}) async-start(bf16[32,16,2048]{2,1,0:T(8,128)(2,1)} %bitcast.9), calls=%async_computation | async-start | bytes 4194304 | tf_op jit(solution)/shard_map/all_to_all | solution.py:96
  13.9 35.4 %collective-permute-start = (bf16[15,512]{1,0:T(8,128)(2,1)S(1)}, bf16[15,512]{1,0:T(8,128)(2,1)S(1)}, u32[]{:S(2)}, u32[]{:S(2)}) collective-permute-start(bf16[15,512]{1,0:T(8,128)(2,1)S(1)} %slice.51), channel_id=1, source_target_pairs={{0,4},{4,8},{8,12},{12,16},{16,20},{20,24},{24,28},{1,5},{5,9},{9,... | collective-permute-start | bytes 46088 | tf_op jit(solution)/shard_map/ppermute | solution.py:12
  51.1 1.6 %copy-start.1 = (f32[1551,512]{1,0:T(8,128)}, f32[1551,512]{1,0:T(8,128)S(1)}, u32[]{:S(2)}) copy-start(f32[1551,512]{1,0:T(8,128)S(1)} %maximum_convert_fusion) | copy-start | bytes 9529348
  76.4 61.9 %all-to-all-start.1 = ((bf16[32,16,2048]{2,1,0:T(8,128)(2,1)}), bf16[32,16,2048]{2,1,0:T(8,128)(2,1)S(1)}, u32[]{:S(2)}, u32[]{:S(2)}) async-start(bf16[32,16,2048]{2,1,0:T(8,128)(2,1)} %bitcast.56), calls=%async_computation.1 | async-start | bytes 4194304 | tf_op jit(solution)/shard_map/all_to_all | solution.py:94
  90.5 1.9 %copy-start.2 = (f32[1551,512]{1,0:T(8,128)S(1)}, f32[1551,512]{1,0:T(8,128)}, u32[]{:S(2)}) copy-start(f32[1551,512]{1,0:T(8,128)} %copy-done.1) | copy-start | bytes 9529348
  90.5 2.9 %copy-start.3 = (f32[1550,512]{1,0:T(8,128)S(1)}, f32[1550,512]{1,0:T(8,128)}, u32[]{:S(2)}) copy-start(f32[1550,512]{1,0:T(8,128)} %slice_add_fusion.1) | copy-start | bytes 9523204
  90.5 2.9 %copy-start.7 = (f32[512]{0:T(512)S(1)}, f32[512]{0:T(512)}, u32[]{:S(2)}) copy-start(f32[512]{0:T(512)} %param.13) | copy-start | bytes 6148
  96.8 1.2 copy-start.4
  98.0 16.2 %collective-permute-start.1 = (bf16[384,512]{1,0:T(8,128)(2,1)}, bf16[384,512]{1,0:T(8,128)(2,1)}, u32[]{:S(2)}, u32[]{:S(2)}) collective-permute-start(bf16[384,512]{1,0:T(8,128)(2,1)} %get-tuple-element.6), channel_id=1, source_target_pairs={{0,1},{1,2},{2,3},{3,0},{4,5},{5,6},{6,7},{7,4},{8,9},{9,10},{10,1... | collective-permute-start | bytes 1179656 | tf_op jit(solution)/shard_map/ppermute | solution.py:127
  98.5 28.6 %collective-permute-start.2 = (bf16[384,512]{1,0:T(8,128)(2,1)S(1)}, bf16[384,512]{1,0:T(8,128)(2,1)}, u32[]{:S(2)}, u32[]{:S(2)}) collective-permute-start(bf16[384,512]{1,0:T(8,128)(2,1)S(1)} %get-tuple-element.5), channel_id=1, source_target_pairs={{0,2},{1,3},{2,0},{3,1},{4,6},{5,7},{6,4},{7,5},{8,10},{9,11},{10,... | collective-permute-start | bytes 1179656 | tf_op jit(solution)/shard_map/ppermute | solution.py:127
  99.7 29.2 %collective-permute-start.3 = (bf16[384,512]{1,0:T(8,128)(2,1)S(1)}, bf16[384,512]{1,0:T(8,128)(2,1)S(1)}, u32[]{:S(2)}, u32[]{:S(2)}) collective-permute-start(bf16[384,512]{1,0:T(8,128)(2,1)S(1)} %get-tuple-element.4), channel_id=1, source_target_pairs={{0,3},{1,0},{2,1},{3,2},{4,7},{5,4},{6,5},{7,6},{8,11},{9,8},{10,9... | collective-permute-start | bytes 1179656 | tf_op jit(solution)/shard_map/ppermute | solution.py:127

commit v2 on v1

--- a/solution.py
+++ b/solution.py
@@ -1,6 +1,10 @@
+import functools
+
 import jax
 import jax.numpy as jnp
 from jax import lax
+from jax.experimental import pallas as pl
+from jax.experimental.pallas import tpu as pltpu
 from jax.sharding import PartitionSpec as P
 
 epsilon = 1e-06
@@ -62,6 +66,117 @@
     return jnp.concatenate(results, axis=1).reshape(received.shape)
 
 
+def send_experts_kernel(
+    n_tp, total, cap, chunks,
+    slots, gate_hbm, up_hbm, down_hbm, landed,
+    gate, up, down, active, outgoing, load_sem, send_sem, recv_sem,
+):
+    loads = [
+        pltpu.make_async_copy(source.at[0], dest, load_sem.at[i])
+        for i, (source, dest) in enumerate(((gate_hbm, gate), (up_hbm, up), (down_hbm, down)))
+    ]
+    for load in loads:
+        load.start()
+    me = lax.axis_index("ep") * n_tp + lax.axis_index("tp")
+    peers = total // chunks
+    rows = peers * cap
+    plane, place = lax.div(me, peers), lax.rem(me, peers)
+    half = lax.rem(plane + chunks // 2, chunks)
+    if chunks == 4:
+        order = [half, 3 - plane, 3 - half, plane]
+    else:
+        order = [lax.rem(plane + c, chunks) for c in range(1, chunks + 1)]
+    ff, width = gate.shape[1], gate.shape[0]
+    tile_f, tile_n = min(ff, 256), min(width, 512)
+
+    def block(ref, owner):
+        return ref.at[pl.ds(pl.multiple_of(owner * cap, cap), cap), :]
+
+    def send(owner):
+        return pltpu.make_async_remote_copy(
+            src_ref=block(outgoing, owner),
+            dst_ref=block(landed, me),
+            send_sem=send_sem.at[owner],
+            recv_sem=recv_sem.at[me],
+            device_id=(lax.div(owner, n_tp), lax.rem(owner, n_tp)),
+            device_id_type=pl.DeviceIdType.MESH,
+        )
+
+    for c in range(chunks):
+        start = pl.multiple_of(order[c] * rows, rows)
+        if c == 0:
+            loads[0].wait()
+            loads[1].wait()
+
+        @pl.loop(0, ff // tile_f)
+        def _(i):
+            cols = pl.ds(pl.multiple_of(i * tile_f, tile_f), tile_f)
+            held = slots[pl.ds(start, rows), :]
+            g = jnp.dot(held, gate[:, cols], preferred_element_type=jnp.float32)
+            u = jnp.dot(held, up[:, cols], preferred_element_type=jnp.float32)
+            active[:, cols] = (g / (1.0 + jnp.exp(-g)) * u).astype(jnp.bfloat16)
+
+        if c == 0:
+            loads[2].wait()
+
+        @pl.loop(0, width // tile_n)
+        def _(i):
+            cols = pl.ds(pl.multiple_of(i * tile_n, tile_n), tile_n)
+            r = jnp.dot(active[...], down[:, cols], preferred_element_type=jnp.float32)
+            outgoing[pl.ds(start, rows), cols] = r.astype(jnp.bfloat16)
+
+        last = c == chunks - 1
+
+        @pl.loop(0, peers - 1 if last else peers)
+        def _(q):
+            turn = lax.rem(place + 1 + q, peers)
+            send(order[c] * peers + turn).start()
+
+    own = pl.ds(pl.multiple_of(me * cap, cap), cap)
+    landed[own, :] = outgoing[own, :]
+
+    @pl.loop(1, total)
+    def _(i):
+        owner = lax.rem(me + i, total)
+        send(owner).wait_send()
+        pltpu.make_async_remote_copy(
+            src_ref=block(outgoing, owner),
+            dst_ref=block(landed, owner),
+            send_sem=send_sem.at[owner],
+            recv_sem=recv_sem.at[owner],
+            device_id=(lax.div(owner, n_tp), lax.rem(owner, n_tp)),
+            device_id_type=pl.DeviceIdType.MESH,
+        ).wait_recv()
+
+
+def send_experts(received, gate_proj, up_proj, down_proj):
+    n_tp = lax.axis_size("tp")
+    total, cap, width = received.shape
+    chunks = 4 if total % 4 == 0 else 1
+    ff = gate_proj.shape[2]
+    vmem, anywhere = pl.BlockSpec(memory_space=pltpu.VMEM), pl.BlockSpec(memory_space=pl.ANY)
+    slots = received.reshape(total * cap, width)
+    return pl.pallas_call(
+        functools.partial(send_experts_kernel, n_tp, total, cap, chunks),
+        out_shape=jax.ShapeDtypeStruct(slots.shape, jnp.bfloat16),
+        in_specs=[vmem, anywhere, anywhere, anywhere],
+        out_specs=vmem,
+        scratch_shapes=[
+            pltpu.VMEM((width, ff), jnp.bfloat16),
+            pltpu.VMEM((width, ff), jnp.bfloat16),
+            pltpu.VMEM((ff, width), jnp.bfloat16),
+            pltpu.VMEM((total // chunks * cap, ff), jnp.bfloat16),
+            pltpu.VMEM(slots.shape, jnp.bfloat16),
+            pltpu.SemaphoreType.DMA((3,)),
+            pltpu.SemaphoreType.DMA((total,)),
+            pltpu.SemaphoreType.DMA((total,)),
+        ],
+        compiler_params=pltpu.CompilerParams(
+            has_side_effects=True, vmem_limit_bytes=60 * 1024 * 1024
+        ),
+    )(slots, gate_proj, up_proj, down_proj)
+
+
 def slot_targets(expert_ids, experts_all, capacity):
     tok_rows, top_count = expert_ids.shape
     experts = lax.iota(jnp.int32, experts_all)[None, :]
@@ -77,7 +192,7 @@
     return targets
 
 
-def route_experts(moe_input, norm_gain, expert_ids, expert_scores, gate_proj, up_proj, down_proj):
+def route_experts(mixed_tokens, moe_input, norm_gain, expert_ids, expert_scores, gate_proj, up_proj, down_proj):
     tok_rows, model_width = moe_input.shape
     top_count = expert_ids.shape[1]
     experts_all = lax.axis_size("ep") * lax.axis_size("tp") * gate_proj.shape[0]
@@ -91,18 +206,14 @@
     fill = sum((slots[:, None] == t[None, :]).astype(jnp.bfloat16) for t in targets)
     outbound = jnp.dot(fill, normed, preferred_element_type=jnp.float32).astype(jnp.bfloat16)
     outbound = outbound.reshape(experts_all, capacity, model_width)
-    returned = lax.all_to_all(
-        expert_block(
-            lax.all_to_all(outbound, ("ep", "tp"), split_axis=0, concat_axis=0, tiled=True),
-            gate_proj,
-            up_proj,
-            down_proj,
-        ),
-        ("ep", "tp"),
-        split_axis=0,
-        concat_axis=0,
-        tiled=True,
-    ).reshape(experts_all * capacity, model_width)
+    received = lax.all_to_all(outbound, ("ep", "tp"), split_axis=0, concat_axis=0, tiled=True)
+    received, mixed_tokens = lax.optimization_barrier((received, mixed_tokens))
+    if capacity % 16 == 0 and gate_proj.shape[0] == 1:
+        returned = send_experts(received, gate_proj, up_proj, down_proj)
+    else:
+        results = expert_block(received, gate_proj, up_proj, down_proj)
+        returned = lax.all_to_all(results, ("ep", "tp"), split_axis=0, concat_axis=0, tiled=True)
+    returned = returned.reshape(experts_all * capacity, model_width)
     weights = expert_scores / jnp.sum(expert_scores, axis=1, keepdims=True)
     spread = sum(
         jnp.where(slots[None, :] == targets[k][:, None], weights[:, k : k + 1], 0.0)
@@ -112,7 +223,7 @@
     fine = (spread - coarse).astype(jnp.bfloat16)
     mixed = jnp.dot(coarse.astype(jnp.bfloat16), returned, preferred_element_type=jnp.float32)
     mixed = mixed + jnp.dot(fine, returned, preferred_element_type=jnp.float32)
-    return mixed.astype(jnp.bfloat16)
+    return mixed_tokens, mixed.astype(jnp.bfloat16)
 
 
 def exchange_groups(hidden):
@@ -147,10 +258,9 @@
     mixed_tokens = jnp.dot(gathered, out_proj, preferred_element_type=jnp.float32).astype(
         jnp.bfloat16
     )
-    mixed_experts = route_experts(
-        moe_input, norm_gain, expert_ids, expert_scores, gate_proj, up_proj, down_proj
-    )
-    return (mixed_tokens, mixed_experts)
+    return route_experts(
+        mixed_tokens, moe_input, norm_gain, expert_ids, expert_scores, gate_proj, up_proj, down_proj
+    )
 
 
 def solution(mesh):

time: 142 us -> 135 us (0.951); the launches traced: 140 us -> 135 us
  Pallas kernels: 0 us -> 63.6 us
  waiting for transfers between devices: 63.4 us -> 27 us
  matrix products: 31.8 us -> 17.8 us
  starting transfers between devices: 21.6 us -> 10.5 us
  other arithmetic: 10.1 us -> 5.17 us
  local copies, waits for them, and re-layouts: 12.2 us -> 9.88 us
    pallas_call x0 -> x1, Pallas kernels: none -> 63.6 us  [send_experts(): pl.pallas_call(functools.partial(send_experts_kernel, n_tp, total, cap, c...]
    ppermute x1, waiting for transfers between devices: 32.1 us -> 0.01 us  [shifted(): lax.ppermute(value, axis, [(source, source + steps) for source in range(f...]
    dot_general x2 -> x0, matrix products: 15.8 us -> none  [the longest x1 9.94 us: expert_block(): result = jnp.dot(active, down_proj[j], preferred_element_type=jnp.float32)]
    all_to_all x1 -> x0, starting transfers between devices: 10.5 us -> none  [route_experts(): lax.all_to_all(expert_block(lax.all_to_all(outbound, ('ep', 'tp'), split_...]
    all_to_all x1, waiting for transfers between devices: 5.68 us -> 0.01 us  [route_experts(): lax.all_to_all(outbound, ('ep', 'tp'), split_axis=0, concat_axis=0, tiled...]
    add x3, other arithmetic: 6.16 us -> 1.25 us  [window_sums(): running = running[stride:] + running[:-stride]]
    unnamed x16 -> x14, local copies, waits for them, and re-layouts: 5.2 us -> 2.76 us
    dot_general x1, matrix products: 0.51 us -> 2.26 us  [route_experts(): jnp.dot(coarse.astype(jnp.bfloat16), returned, preferred_element_type=jnp...]
  transfers between devices with their start and end apart: 6 -> 5, of which waited for: 4 -> 2; matrix products, arithmetic and copies ran while one was open for 18% -> 19% of each run, Pallas kernels for 0% -> 0%
where the time goes in v2:
time: 135 us
  Pallas kernels  63.6 us (47%)
  waiting for transfers between devices  27 us (20%)
  matrix products  17.8 us (13%)
  starting transfers between devices  10.5 us (8%)
  local copies, waits for them, and re-layouts  9.88 us (7%)
  other arithmetic  5.17 us (4%)
    pallas_call x1, Pallas kernels, send_experts(): pl.pallas_call(functools.partial(send_experts_kernel, n_tp, total, cap, c...  63.6 us
    ppermute x3, waiting for transfers between devices, exchange_groups(): lax.ppermute(block, 'tp', [(i, (i + step) % count) for i in range(count)])  27 us
    dot_general x1, matrix products, body(): jnp.dot(gathered, out_proj, preferred_element_type=jnp.float32)  8.42 us
    all_to_all x1, starting transfers between devices, route_experts(): lax.all_to_all(outbound, ('ep', 'tp'), split_axis=0, concat_axis=0, tiled...  5.62 us
    dynamic_update_slice x3, local copies, waits for them, and re-layouts, exchange_groups(): gathered = lax.dynamic_update_slice(gathered, block, (0, source * width))  4.47 us
    dot_general x1, matrix products, route_experts(): jnp.dot(fill, normed, preferred_element_type=jnp.float32)  3.21 us
    ppermute x1, starting transfers between devices, shifted(): lax.ppermute(value, axis, [(source, source + steps) for source in range(f...  3.14 us
    unnamed x14, local copies, waits for them, and re-layouts  2.76 us
  transfers between devices with their start and end apart: 5, of which 2 were waited for; matrix products, arithmetic and copies ran while one was open for 19% of the time, Pallas kernels for 0%

profile of v2, /device:TPU:11, one launch (start us, length us, event | category | flops | bytes accessed | tf_op | source)
XLA Modules:
  0.0 134.8 jit_solution(2210036014247597929)
XLA Ops:
  0.6 0.0 copy-start
  0.6 0.8 slice.53
  1.4 3.1 %collective-permute-start = (bf16[15,512]{1,0:T(8,128)(2,1)S(1)}, bf16[15,512]{1,0:T(8,128)(2,1)S(1)}, u32[]{:S(2)}, u32[]{:S(2)}) collective-permute-start(bf16[15,512]{1,0:T(8,128)(2,1)S(1)} %slice.53), channel_id=1, source_target_pairs={{0,4},{4,8},{8,12},{12,16},{16,20},{20,24},{24,28},{1,5},{5,9},{9,... | collective-permute-start | bytes 46088 | tf_op jit(solution)/shard_map/ppermute | solution.py:16
  4.6 0.8 slice_bitcast_fusion.3
  5.3 1.2 fusion.9
  6.6 0.2 select_reduce_fusion.1
  6.7 0.8 convert_add_fusion.1
  7.5 3.2 %convolution_convert_fusion = bf16[512,2048]{1,0:T(8,128)(2,1)} fusion(bf16[128,2048]{1,0:T(8,128)(2,1)} %param.15, f32[2048]{0:T(1024)} %param.16, f32[128]{0:T(128)S(1)} %add_rsqrt_fusion, s32[128]{0:T(128)S(1)} %get-tuple-element.17, s32[128]{0:T(128)S(1)} %get-tuple-element.16), kind=kOutput, calls=%fused_computation.14 | convolution fusion | flops 271056896 | bytes 2631168 | tf_op jit(solution)/shard_map/dot_general | solution.py:207
  10.7 5.6 %all-to-all-start = ((bf16[32,16,2048]{2,1,0:T(8,128)(2,1)}), bf16[32,16,2048]{2,1,0:T(8,128)(2,1)S(1)}, u32[]{:S(2)}, u32[]{:S(2)}) async-start(bf16[32,16,2048]{2,1,0:T(8,128)(2,1)} %bitcast.2), calls=%async_computation | async-start | bytes 4194304 | tf_op jit(solution)/shard_map/all_to_all | solution.py:209
  16.5 0.0 collective-permute-done
  16.5 1.9 %maximum_convert_fusion = f32[1551,512]{1,0:T(8,128)S(1)} fusion(bf16[1536,512]{1,0:T(8,128)(2,1)} %param.11, bf16[15,512]{1,0:T(8,128)(2,1)S(1)} %collective-permute-done), kind=kLoop, calls=%fused_computation.19 | loop fusion | flops 3176448 | bytes 4764672 | tf_op jit(solution)/shard_map/convert_element_type | solution.py:36
  18.4 0.4 slice_add_fusion.1
  18.8 0.4 slice_add_fusion
  19.2 0.0 copy-start.6
  19.2 0.4 slice_add_fusion.2
  19.7 0.2 copy-done.6
  19.9 2.4 %fusion.6 = bf16[1536,512]{1,0:T(8,128)(2,1)S(1)} fusion(f32[512]{0:T(512)S(1)} %copy-done.6, f32[1551,512]{1,0:T(8,128)S(1)} %maximum_convert_fusion, f32[1544,512]{1,0:T(8,128)S(1)} %slice_add_fusion.2, f32[1548,512]{1,0:T(8,128)S(1)} %slice_add_fusion, f32[1550,512]{1,0:T(8,128)S(1)} %slice_add_fusion.1, f32[1536]{0:T(1024)S(1)} %minimum_convert_fusion, ...), kind=kOutput, calls=%fused_computation.15 | convolution fusion | flops 815529984 | bytes 17836036 | tf_op jit(solution)/shard_map/dot_general | solution.py:49
  22.3 0.2 broadcast_in_dim.54
  22.5 0.9 constant_dynamic-slice_fusion
  23.4 1.1 copy-done.3
  24.5 0.5 collective-permute-start.1
  25.1 1.2 collective-permute-start.2
  26.3 13.1 %collective-permute-done.1 = bf16[384,512]{1,0:T(8,128)(2,1)} collective-permute-done((bf16[384,512]{1,0:T(8,128)(2,1)}, bf16[384,512]{1,0:T(8,128)(2,1)}, u32[]{:S(2)}, u32[]{:S(2)}) %collective-permute-start.1) | collective-permute-done | bytes 393248 | tf_op jit(solution)/shard_map/ppermute | solution.py:238
  39.4 1.8 %constant_dynamic-update-slice_fusion.1 = bf16[384,2048]{1,0:T(8,128)(2,1)} fusion(bf16[384,2048]{1,0:T(8,128)(2,1)} %copy-done.3, bf16[384,512]{1,0:T(8,128)(2,1)} %collective-permute-done.1, s32[]{:T(128)S(6)} %select_n.77), kind=kLoop, calls=%fused_computation.68 | loop fusion | bytes 786436 | tf_op jit(solution)/shard_map/dynamic_update_slice | solution.py:239
  41.2 13.9 %collective-permute-done.2 = bf16[384,512]{1,0:T(8,128)(2,1)} collective-permute-done((bf16[384,512]{1,0:T(8,128)(2,1)S(1)}, bf16[384,512]{1,0:T(8,128)(2,1)}, u32[]{:S(2)}, u32[]{:S(2)}) %collective-permute-start.2) | collective-permute-done | bytes 393248 | tf_op jit(solution)/shard_map/ppermute | solution.py:238
  55.1 1.8 %constant_dynamic-update-slice_fusion = bf16[384,2048]{1,0:T(8,128)(2,1)} fusion(bf16[384,2048]{1,0:T(8,128)(2,1)} %constant_dynamic-update-slice_fusion.1, bf16[384,512]{1,0:T(8,128)(2,1)} %collective-permute-done.2, s32[]{:T(128)S(6)} %select_n.79), kind=kLoop, calls=%fused_computation.66 | loop fusion | bytes 786436 | tf_op jit(solution)/shard_map/dynamic_update_slice | solution.py:239
  56.9 0.8 constant_dynamic-update-slice_fusion.2
  57.8 8.4 %convolution_convert_fusion.1 = bf16[384,2048]{1,0:T(8,128)(2,1)} fusion(bf16[384,2048]{1,0:T(8,128)(2,1)} %constant_dynamic-update-slice_fusion.2, bf16[2048,2048]{1,0:T(8,128)(2,1)} %param.14), kind=kOutput, calls=%fused_computation.16 | convolution fusion | flops 3222011904 | bytes 11534336 | tf_op jit(solution)/shard_map/dot_general | solution.py:258
  66.2 1.3 copy-done.2
  67.5 63.6 %shard_map.122 = bf16[512,2048]{1,0:T(8,128)(2,1)} custom-call(bf16[512,2048]{1,0:T(8,128)(2,1)} %bitcast.33, bf16[1,2048,1024]{2,1,0:T(8,128)(2,1)} %gate_hbm.1, bf16[1,2048,1024]{2,1,0:T(8,128)(2,1)} %up_hbm.1, bf16[1,1024,2048]{2,1,0:T(8,128)(2,1)} %down_hbm.1), custom_call_target="tpu_custom_call" | custom-call | tf_op jit(solution)/shard_map/pallas_call | solution.py:159
  131.2 2.3 %fusion.20 = f32[128,2048]{1,0:T(8,128)S(1)} fusion(bf16[512,2048]{1,0:T(8,128)(2,1)} %shard_map.122, f32[128]{0:T(128)S(1)} %get-tuple-element.15, s32[128]{0:T(128)S(1)} %get-tuple-element.13, f32[128]{0:T(128)S(1)} %get-tuple-element.14, s32[128]{0:T(128)S(1)} %get-tuple-element.12), kind=kOutput, calls=%fused_computation.39 | convolution fusion | flops 268894208 | bytes 3147776 | tf_op jit(solution)/shard_map/dot_general | solution.py:224
  133.5 1.3 fusion.7
  (18 shorter events, 0.1 us)
Async XLA Ops:
  0.6 19.0 %copy-start = (bf16[1,512,512]{2,1,0:T(8,128)(2,1)S(1)}, bf16[1,512,512]{2,1,0:T(8,128)(2,1)}, u32[]{:S(2)}) copy-start(bf16[1,512,512]{2,1,0:T(8,128)(2,1)} %param.12) | copy-start | bytes 1572868
  1.4 15.1 %collective-permute-start = (bf16[15,512]{1,0:T(8,128)(2,1)S(1)}, bf16[15,512]{1,0:T(8,128)(2,1)S(1)}, u32[]{:S(2)}, u32[]{:S(2)}) collective-permute-start(bf16[15,512]{1,0:T(8,128)(2,1)S(1)} %slice.53), channel_id=1, source_target_pairs={{0,4},{4,8},{8,12},{12,16},{16,20},{20,24},{24,28},{1,5},{5,9},{9,... | collective-permute-start | bytes 46088 | tf_op jit(solution)/shard_map/ppermute | solution.py:16
  7.5 8.9 %copy-start.4 = (s32[128,2]{0,1:T(2,128)S(1)}, s32[128,2]{0,1:T(2,128)}, u32[]{:S(2)}) copy-start(s32[128,2]{0,1:T(2,128)} %param.17) | copy-start | bytes 3076
  7.5 8.9 %copy-start.5 = (f32[128,2]{0,1:T(2,128)S(1)}, f32[128,2]{0,1:T(2,128)}, u32[]{:S(2)}) copy-start(f32[128,2]{0,1:T(2,128)} %param.18) | copy-start | bytes 3076
  10.7 55.5 %all-to-all-start = ((bf16[32,16,2048]{2,1,0:T(8,128)(2,1)}), bf16[32,16,2048]{2,1,0:T(8,128)(2,1)S(1)}, u32[]{:S(2)}, u32[]{:S(2)}) async-start(bf16[32,16,2048]{2,1,0:T(8,128)(2,1)} %bitcast.2), calls=%async_computation | async-start | bytes 4194304 | tf_op jit(solution)/shard_map/all_to_all | solution.py:209
  19.2 0.7 copy-start.6
  23.4 1.1 copy-start.3
  24.5 14.8 %collective-permute-start.1 = (bf16[384,512]{1,0:T(8,128)(2,1)}, bf16[384,512]{1,0:T(8,128)(2,1)}, u32[]{:S(2)}, u32[]{:S(2)}) collective-permute-start(bf16[384,512]{1,0:T(8,128)(2,1)} %get-tuple-element.10), channel_id=1, source_target_pairs={{0,1},{1,2},{2,3},{3,0},{4,5},{5,6},{6,7},{7,4},{8,9},{9,10},{10,1... | collective-permute-start | bytes 1179656 | tf_op jit(solution)/shard_map/ppermute | solution.py:238
  25.1 30.0 %collective-permute-start.2 = (bf16[384,512]{1,0:T(8,128)(2,1)S(1)}, bf16[384,512]{1,0:T(8,128)(2,1)}, u32[]{:S(2)}, u32[]{:S(2)}) collective-permute-start(bf16[384,512]{1,0:T(8,128)(2,1)S(1)} %get-tuple-element.9), channel_id=1, source_target_pairs={{0,2},{1,3},{2,0},{3,1},{4,6},{5,7},{6,4},{7,5},{8,10},{9,11},{10,... | collective-permute-start | bytes 1179656 | tf_op jit(solution)/shard_map/ppermute | solution.py:238
  26.3 30.7 %collective-permute-start.3 = (bf16[384,512]{1,0:T(8,128)(2,1)S(1)}, bf16[384,512]{1,0:T(8,128)(2,1)S(1)}, u32[]{:S(2)}, u32[]{:S(2)}) collective-permute-start(bf16[384,512]{1,0:T(8,128)(2,1)S(1)} %get-tuple-element.8), channel_id=1, source_target_pairs={{0,3},{1,0},{2,1},{3,2},{4,7},{5,4},{6,5},{7,6},{8,11},{9,8},{10,9... | collective-permute-start | bytes 1179656 | tf_op jit(solution)/shard_map/ppermute | solution.py:238
  66.2 1.3 %copy-start.2 = (bf16[32,16,2048]{2,1,0:T(8,128)(2,1)}, bf16[32,16,2048]{2,1,0:T(8,128)(2,1)S(1)}, u32[]{:S(2)}) copy-start(bf16[32,16,2048]{2,1,0:T(8,128)(2,1)S(1)} %all-to-all-done) | copy-start | bytes 6291460
  131.2 2.3 %copy-start.1 = (bf16[512,2048]{1,0:T(8,128)(2,1)S(1)}, bf16[512,2048]{1,0:T(8,128)(2,1)}, u32[]{:S(2)}) copy-start(bf16[512,2048]{1,0:T(8,128)(2,1)} %shard_map.122) | copy-start | bytes 6291460

commit v3 on v2

--- a/solution.py
+++ b/solution.py
@@ -68,16 +68,29 @@
 
 def send_experts_kernel(
     n_tp, total, cap, chunks,
-    slots, gate_hbm, up_hbm, down_hbm, landed,
-    gate, up, down, active, outgoing, load_sem, send_sem, recv_sem,
+    slots, gathered, gate_hbm, up_hbm, down_hbm, proj_hbm, landed, mixed,
+    gate, up, down, proj, active, outgoing, load_sem, send_sem, recv_sem,
 ):
     loads = [
         pltpu.make_async_copy(source.at[0], dest, load_sem.at[i])
         for i, (source, dest) in enumerate(((gate_hbm, gate), (up_hbm, up), (down_hbm, down)))
     ]
+    loads.append(pltpu.make_async_copy(proj_hbm, proj, load_sem.at[3]))
     for load in loads:
         load.start()
     me = lax.axis_index("ep") * n_tp + lax.axis_index("tp")
+    barrier = pltpu.get_barrier_semaphore()
+
+    @pl.loop(1, total)
+    def _(i):
+        other = lax.rem(me + i, total)
+        pl.semaphore_signal(
+            barrier,
+            inc=1,
+            device_id=(lax.div(other, n_tp), lax.rem(other, n_tp)),
+            device_id_type=pl.DeviceIdType.MESH,
+        )
+
     peers = total // chunks
     rows = peers * cap
     plane, place = lax.div(me, peers), lax.rem(me, peers)
@@ -125,6 +138,8 @@
             r = jnp.dot(active[...], down[:, cols], preferred_element_type=jnp.float32)
             outgoing[pl.ds(start, rows), cols] = r.astype(jnp.bfloat16)
 
+        if c == 0:
+            pl.semaphore_wait(barrier, total - 1)
         last = c == chunks - 1
 
         @pl.loop(0, peers - 1 if last else peers)
@@ -134,6 +149,13 @@
 
     own = pl.ds(pl.multiple_of(me * cap, cap), cap)
     landed[own, :] = outgoing[own, :]
+    loads[3].wait()
+
+    @pl.loop(0, width // tile_n)
+    def _(i):
+        cols = pl.ds(pl.multiple_of(i * tile_n, tile_n), tile_n)
+        r = jnp.dot(gathered[...], proj[:, cols], preferred_element_type=jnp.float32)
+        mixed[:, cols] = r.astype(jnp.bfloat16)
 
     @pl.loop(1, total)
     def _(i):
@@ -149,7 +171,7 @@
         ).wait_recv()
 
 
-def send_experts(received, gate_proj, up_proj, down_proj):
+def send_experts(received, gathered, out_proj, gate_proj, up_proj, down_proj):
     n_tp = lax.axis_size("tp")
     total, cap, width = received.shape
     chunks = 4 if total % 4 == 0 else 1
@@ -158,23 +180,27 @@
     slots = received.reshape(total * cap, width)
     return pl.pallas_call(
         functools.partial(send_experts_kernel, n_tp, total, cap, chunks),
-        out_shape=jax.ShapeDtypeStruct(slots.shape, jnp.bfloat16),
-        in_specs=[vmem, anywhere, anywhere, anywhere],
-        out_specs=vmem,
+        out_shape=(
+            jax.ShapeDtypeStruct(slots.shape, jnp.bfloat16),
+            jax.ShapeDtypeStruct((gathered.shape[0], out_proj.shape[1]), jnp.bfloat16),
+        ),
+        in_specs=[vmem, vmem] + [anywhere] * 4,
+        out_specs=(vmem, vmem),
         scratch_shapes=[
             pltpu.VMEM((width, ff), jnp.bfloat16),
             pltpu.VMEM((width, ff), jnp.bfloat16),
             pltpu.VMEM((ff, width), jnp.bfloat16),
+            pltpu.VMEM(out_proj.shape, jnp.bfloat16),
             pltpu.VMEM((total // chunks * cap, ff), jnp.bfloat16),
             pltpu.VMEM(slots.shape, jnp.bfloat16),
-            pltpu.SemaphoreType.DMA((3,)),
+            pltpu.SemaphoreType.DMA((4,)),
             pltpu.SemaphoreType.DMA((total,)),
             pltpu.SemaphoreType.DMA((total,)),
         ],
         compiler_params=pltpu.CompilerParams(
-            has_side_effects=True, vmem_limit_bytes=60 * 1024 * 1024
+            collective_id=0, has_side_effects=True, vmem_limit_bytes=60 * 1024 * 1024
         ),
-    )(slots, gate_proj, up_proj, down_proj)
+    )(slots, gathered, gate_proj, up_proj, down_proj, out_proj)
 
 
 def slot_targets(expert_ids, experts_all, capacity):
@@ -192,7 +218,19 @@
     return targets
 
 
-def route_experts(mixed_tokens, moe_input, norm_gain, expert_ids, expert_scores, gate_proj, up_proj, down_proj):
+def body(
+    pool_input,
+    group_mix,
+    group_scale,
+    out_proj,
+    moe_input,
+    norm_gain,
+    expert_ids,
+    expert_scores,
+    gate_proj,
+    up_proj,
+    down_proj,
+):
     tok_rows, model_width = moe_input.shape
     top_count = expert_ids.shape[1]
     experts_all = lax.axis_size("ep") * lax.axis_size("tp") * gate_proj.shape[0]
@@ -206,13 +244,19 @@
     fill = sum((slots[:, None] == t[None, :]).astype(jnp.bfloat16) for t in targets)
     outbound = jnp.dot(fill, normed, preferred_element_type=jnp.float32).astype(jnp.bfloat16)
     outbound = outbound.reshape(experts_all, capacity, model_width)
+    outbound, pool_input = lax.optimization_barrier((outbound, pool_input))
     received = lax.all_to_all(outbound, ("ep", "tp"), split_axis=0, concat_axis=0, tiled=True)
-    received, mixed_tokens = lax.optimization_barrier((received, mixed_tokens))
+    gathered = exchange_groups(pool_groups(pool_input, group_mix, group_scale))
+    received, gathered = lax.optimization_barrier((received, gathered))
     if capacity % 16 == 0 and gate_proj.shape[0] == 1:
-        returned = send_experts(received, gate_proj, up_proj, down_proj)
+        returned, mixed_tokens = send_experts(
+            received, gathered, out_proj, gate_proj, up_proj, down_proj
+        )
     else:
         results = expert_block(received, gate_proj, up_proj, down_proj)
         returned = lax.all_to_all(results, ("ep", "tp"), split_axis=0, concat_axis=0, tiled=True)
+        mixed_tokens = jnp.dot(gathered, out_proj, preferred_element_type=jnp.float32)
+        mixed_tokens = mixed_tokens.astype(jnp.bfloat16)
     returned = returned.reshape(experts_all * capacity, model_width)
     weights = expert_scores / jnp.sum(expert_scores, axis=1, keepdims=True)
     spread = sum(
@@ -238,29 +282,6 @@
             block = lax.ppermute(block, "tp", [(i, (i + step) % count) for i in range(count)])
         gathered = lax.dynamic_update_slice(gathered, block, (0, source * width))
     return gathered
-
-
-def body(
-    pool_input,
-    group_mix,
-    group_scale,
-    out_proj,
-    moe_input,
-    norm_gain,
-    expert_ids,
-    expert_scores,
-    gate_proj,
-    up_proj,
-    down_proj,
-):
-    hidden = pool_groups(pool_input, group_mix, group_scale)
-    gathered = exchange_groups(hidden)
-    mixed_tokens = jnp.dot(gathered, out_proj, preferred_element_type=jnp.float32).astype(
-        jnp.bfloat16
-    )
-    return route_experts(
-        mixed_tokens, moe_input, norm_gain, expert_ids, expert_scores, gate_proj, up_proj, down_proj
-    )
 
 
 def solution(mesh):

time: 135 us -> 152 us (1.13)
  waiting for transfers between devices: 27 us -> 48.1 us
  matrix products: 17.8 us -> 9.26 us
    ppermute x1, waiting for transfers between devices: 0.01 us -> 32.1 us  [shifted(): lax.ppermute(value, axis, [(source, source + steps) for source in range(f...]
    ppermute x3, waiting for transfers between devices: 27 us -> 16 us  [exchange_groups(): lax.ppermute(block, 'tp', [(i, (i + step) % count) for i in range(count)])]
    dot_general x4 -> x3, matrix products: 15.2 us -> 6.78 us  [the longest x1 3.21 us: body(): jnp.dot(fill, normed, preferred_element_type=jnp.float32)]
  transfers between devices with their start and end apart: 5 -> 5, of which waited for: 2 -> 3; matrix products, arithmetic and copies ran while one was open for 19% -> 9% of each run, Pallas kernels for 0% -> 0%
where the time goes in v3:
time: 152 us; the launch traced here: 151 us
  Pallas kernels  64.9 us (43%)
  waiting for transfers between devices  48.1 us (32%)
  starting transfers between devices  11.7 us (8%)
  local copies, waits for them, and re-layouts  10.9 us (7%)
  matrix products  9.26 us (6%)
  other arithmetic  5.22 us (3%)
    pallas_call x1, Pallas kernels, send_experts(): pl.pallas_call(functools.partial(send_experts_kernel, n_tp, total, cap, c...  64.9 us
    ppermute x1, waiting for transfers between devices, shifted(): lax.ppermute(value, axis, [(source, source + steps) for source in range(f...  32.1 us
    ppermute x3, waiting for transfers between devices, exchange_groups(): lax.ppermute(block, 'tp', [(i, (i + step) % count) for i in range(count)])  16 us
    all_to_all x1, starting transfers between devices, body(): lax.all_to_all(outbound, ('ep', 'tp'), split_axis=0, concat_axis=0, tiled...  6.3 us
    dynamic_update_slice x3, local copies, waits for them, and re-layouts, exchange_groups(): gathered = lax.dynamic_update_slice(gathered, block, (0, source * width))  4.3 us
    dot_general x1, matrix products, body(): jnp.dot(fill, normed, preferred_element_type=jnp.float32)  3.21 us
    ppermute x1, starting transfers between devices, shifted(): lax.ppermute(value, axis, [(source, source + steps) for source in range(f...  3.08 us
  transfers between devices with their start and end apart: 5, of which 3 were waited for; matrix products, arithmetic and copies ran while one was open for 9% of the time, Pallas kernels for 0%

profile of v3, /device:TPU:11, one launch (start us, length us, event | category | flops | bytes accessed | tf_op | source)
XLA Modules:
  0.0 150.9 jit_solution(16356867126382344069)
XLA Ops:
  0.6 0.0 copy-start
  0.6 1.3 fusion.9
  1.9 0.8 slice_bitcast_fusion.3
  2.7 0.2 select_reduce_fusion.1
  2.9 0.8 convert_add_fusion.1
  3.6 3.2 %convolution_convert_fusion = bf16[512,2048]{1,0:T(8,128)(2,1)} fusion(bf16[128,2048]{1,0:T(8,128)(2,1)} %param.15, f32[2048]{0:T(1024)} %param.16, f32[128]{0:T(128)S(1)} %add_rsqrt_fusion, s32[128]{0:T(128)S(1)} %get-tuple-element.25, s32[128]{0:T(128)S(1)} %get-tuple-element.24), kind=kOutput, calls=%fused_computation.14 | convolution fusion | flops 271056896 | bytes 2631168 | tf_op jit(solution)/shard_map/dot_general | solution.py:245
  6.9 6.3 %all-to-all-start = ((bf16[32,16,2048]{2,1,0:T(8,128)(2,1)}), bf16[32,16,2048]{2,1,0:T(8,128)(2,1)S(1)}, u32[]{:S(2)}, u32[]{:S(2)}) async-start(bf16[32,16,2048]{2,1,0:T(8,128)(2,1)} %bitcast.32), calls=%async_computation | async-start | bytes 4194304 | tf_op jit(solution)/shard_map/all_to_all | solution.py:248
  13.2 0.7 slice.53
  13.9 3.1 %collective-permute-start = (bf16[15,512]{1,0:T(8,128)(2,1)S(1)}, bf16[15,512]{1,0:T(8,128)(2,1)S(1)}, u32[]{:S(2)}, u32[]{:S(2)}) collective-permute-start(bf16[15,512]{1,0:T(8,128)(2,1)S(1)} %slice.53), channel_id=1, source_target_pairs={{0,4},{4,8},{8,12},{12,16},{16,20},{20,24},{24,28},{1,5},{5,9},{9,... | collective-permute-start | bytes 46088 | tf_op jit(solution)/shard_map/ppermute | solution.py:16
  17.1 32.1 %collective-permute-done = bf16[15,512]{1,0:T(8,128)(2,1)S(1)} collective-permute-done((bf16[15,512]{1,0:T(8,128)(2,1)S(1)}, bf16[15,512]{1,0:T(8,128)(2,1)S(1)}, u32[]{:S(2)}, u32[]{:S(2)}) %collective-permute-start) | collective-permute-done | bytes 15392 | tf_op jit(solution)/shard_map/ppermute | solution.py:16
  49.3 1.9 %maximum_convert_fusion = f32[1551,512]{1,0:T(8,128)S(1)} fusion(bf16[1536,512]{1,0:T(8,128)(2,1)} %param.11, bf16[15,512]{1,0:T(8,128)(2,1)S(1)} %collective-permute-done), kind=kLoop, calls=%fused_computation.18 | loop fusion | flops 3176448 | bytes 4764672 | tf_op jit(solution)/shard_map/convert_element_type | solution.py:36
  51.1 0.4 slice_add_fusion.1
  51.6 0.4 slice_add_fusion
  52.0 0.0 copy-start.6
  52.0 0.4 slice_add_fusion.2
  52.4 0.2 copy-done.6
  52.7 2.3 %fusion.6 = bf16[1536,512]{1,0:T(8,128)(2,1)S(1)} fusion(f32[512]{0:T(512)S(1)} %copy-done.6, f32[1551,512]{1,0:T(8,128)S(1)} %maximum_convert_fusion, f32[1544,512]{1,0:T(8,128)S(1)} %slice_add_fusion.2, f32[1548,512]{1,0:T(8,128)S(1)} %slice_add_fusion, f32[1550,512]{1,0:T(8,128)S(1)} %slice_add_fusion.1, f32[1536]{0:T(1024)S(1)} %minimum_convert_fusion, ...), kind=kOutput, calls=%fused_computation.15 | convolution fusion | flops 815529984 | bytes 17836036 | tf_op jit(solution)/shard_map/dot_general | solution.py:49
  55.0 1.3 broadcast_in_dim.54
  56.3 1.0 constant_dynamic-slice_fusion
  57.3 1.2 collective-permute-start.1
  58.6 1.1 collective-permute-start.2
  59.7 0.0 collective-permute-start.3
  59.7 7.8 %collective-permute-done.1 = bf16[384,512]{1,0:T(8,128)(2,1)} collective-permute-done((bf16[384,512]{1,0:T(8,128)(2,1)}, bf16[384,512]{1,0:T(8,128)(2,1)}, u32[]{:S(2)}, u32[]{:S(2)}) %collective-permute-start.1) | collective-permute-done | bytes 393248 | tf_op jit(solution)/shard_map/ppermute | solution.py:282
  67.5 1.8 %constant_dynamic-update-slice_fusion.1 = bf16[384,2048]{1,0:T(8,128)(2,1)} fusion(bf16[384,2048]{1,0:T(8,128)(2,1)} %get-tuple-element.19, bf16[384,512]{1,0:T(8,128)(2,1)} %collective-permute-done.1, s32[]{:T(128)S(6)} %select_n.77), kind=kLoop, calls=%fused_computation.67 | loop fusion | bytes 786436 | tf_op jit(solution)/shard_map/dynamic_update_slice | solution.py:283
  69.2 8.2 %collective-permute-done.2 = bf16[384,512]{1,0:T(8,128)(2,1)} collective-permute-done((bf16[384,512]{1,0:T(8,128)(2,1)S(1)}, bf16[384,512]{1,0:T(8,128)(2,1)}, u32[]{:S(2)}, u32[]{:S(2)}) %collective-permute-start.2) | collective-permute-done | bytes 393248 | tf_op jit(solution)/shard_map/ppermute | solution.py:282
  77.4 1.8 %constant_dynamic-update-slice_fusion = bf16[384,2048]{1,0:T(8,128)(2,1)} fusion(bf16[384,2048]{1,0:T(8,128)(2,1)} %constant_dynamic-update-slice_fusion.1, bf16[384,512]{1,0:T(8,128)(2,1)} %collective-permute-done.2, s32[]{:T(128)S(6)} %select_n.79), kind=kLoop, calls=%fused_computation.65 | loop fusion | bytes 786436 | tf_op jit(solution)/shard_map/dynamic_update_slice | solution.py:283
  79.2 0.8 constant_dynamic-update-slice_fusion.2.gathered
  80.0 1.3 copy-done.1
  81.3 64.9 %shard_map.122 = (bf16[512,2048]{1,0:T(8,128)(2,1)}, bf16[384,2048]{1,0:T(8,128)(2,1)}) custom-call(bf16[512,2048]{1,0:T(8,128)(2,1)} %bitcast.31, bf16[384,2048]{1,0:T(8,128)(2,1)} %constant_dynamic-update-slice_fusion.2.gathered, bf16[1,2048,1024]{2,1,0:T(8,128)(2,1)} %gate_hbm.1, bf16[1,2048,1024]{2,1,0:T(8,128)(2,1)} %up_hbm.1, ...), custom_call_target="tpu_custom_call" | custom-call | tf_op jit(solution)/shard_map/pallas_call | solution.py:181
  146.2 2.3 %fusion.20 = f32[128,2048]{1,0:T(8,128)S(1)} fusion(bf16[512,2048]{1,0:T(8,128)(2,1)} %get-tuple-element.13, f32[128]{0:T(128)S(1)} %get-tuple-element.23, s32[128]{0:T(128)S(1)} %get-tuple-element.21, f32[128]{0:T(128)S(1)} %get-tuple-element.22, s32[128]{0:T(128)S(1)} %get-tuple-element.20), kind=kOutput, calls=%fused_computation.38 | convolution fusion | flops 268894208 | bytes 3147776 | tf_op jit(solution)/shard_map/dot_general | solution.py:268
  148.5 1.3 fusion.7
  149.8 1.1 copy.18
  (18 shorter events, 0.1 us)
Async XLA Ops:
  0.6 51.8 %copy-start = (bf16[1,512,512]{2,1,0:T(8,128)(2,1)S(1)}, bf16[1,512,512]{2,1,0:T(8,128)(2,1)}, u32[]{:S(2)}) copy-start(bf16[1,512,512]{2,1,0:T(8,128)(2,1)} %param.12) | copy-start | bytes 1572868
  3.6 13.3 %copy-start.4 = (s32[128,2]{0,1:T(2,128)S(1)}, s32[128,2]{0,1:T(2,128)}, u32[]{:S(2)}) copy-start(s32[128,2]{0,1:T(2,128)} %param.17) | copy-start | bytes 3076
  3.6 13.4 %copy-start.5 = (f32[128,2]{0,1:T(2,128)S(1)}, f32[128,2]{0,1:T(2,128)}, u32[]{:S(2)}) copy-start(f32[128,2]{0,1:T(2,128)} %param.18) | copy-start | bytes 3076
  6.9 73.1 %all-to-all-start = ((bf16[32,16,2048]{2,1,0:T(8,128)(2,1)}), bf16[32,16,2048]{2,1,0:T(8,128)(2,1)S(1)}, u32[]{:S(2)}, u32[]{:S(2)}) async-start(bf16[32,16,2048]{2,1,0:T(8,128)(2,1)} %bitcast.32), calls=%async_computation | async-start | bytes 4194304 | tf_op jit(solution)/shard_map/all_to_all | solution.py:248
  13.9 35.4 %collective-permute-start = (bf16[15,512]{1,0:T(8,128)(2,1)S(1)}, bf16[15,512]{1,0:T(8,128)(2,1)S(1)}, u32[]{:S(2)}, u32[]{:S(2)}) collective-permute-start(bf16[15,512]{1,0:T(8,128)(2,1)S(1)} %slice.53), channel_id=1, source_target_pairs={{0,4},{4,8},{8,12},{12,16},{16,20},{20,24},{24,28},{1,5},{5,9},{9,... | collective-permute-start | bytes 46088 | tf_op jit(solution)/shard_map/ppermute | solution.py:16
  52.0 0.7 copy-start.6
  57.3 10.1 %collective-permute-start.1 = (bf16[384,512]{1,0:T(8,128)(2,1)}, bf16[384,512]{1,0:T(8,128)(2,1)}, u32[]{:S(2)}, u32[]{:S(2)}) collective-permute-start(bf16[384,512]{1,0:T(8,128)(2,1)} %get-tuple-element.18), channel_id=1, source_target_pairs={{0,1},{1,2},{2,3},{3,0},{4,5},{5,6},{6,7},{7,4},{8,9},{9,10},{10,1... | collective-permute-start | bytes 1179656 | tf_op jit(solution)/shard_map/ppermute | solution.py:282
  58.6 18.8 %collective-permute-start.2 = (bf16[384,512]{1,0:T(8,128)(2,1)S(1)}, bf16[384,512]{1,0:T(8,128)(2,1)}, u32[]{:S(2)}, u32[]{:S(2)}) collective-permute-start(bf16[384,512]{1,0:T(8,128)(2,1)S(1)} %get-tuple-element.17), channel_id=1, source_target_pairs={{0,2},{1,3},{2,0},{3,1},{4,6},{5,7},{6,4},{7,5},{8,10},{9,11},{10,... | collective-permute-start | bytes 1179656 | tf_op jit(solution)/shard_map/ppermute | solution.py:282
  59.7 19.5 %collective-permute-start.3 = (bf16[384,512]{1,0:T(8,128)(2,1)S(1)}, bf16[384,512]{1,0:T(8,128)(2,1)S(1)}, u32[]{:S(2)}, u32[]{:S(2)}) collective-permute-start(bf16[384,512]{1,0:T(8,128)(2,1)S(1)} %get-tuple-element.16), channel_id=1, source_target_pairs={{0,3},{1,0},{2,1},{3,2},{4,7},{5,4},{6,5},{7,6},{8,11},{9,8},{10,9... | collective-permute-start | bytes 1179656 | tf_op jit(solution)/shard_map/ppermute | solution.py:282
  80.0 1.3 copy-start.1
  146.2 2.3 %copy-start.2 = (bf16[512,2048]{1,0:T(8,128)(2,1)S(1)}, bf16[512,2048]{1,0:T(8,128)(2,1)}, u32[]{:S(2)}) copy-start(bf16[512,2048]{1,0:T(8,128)(2,1)} %get-tuple-element.13) | copy-start | bytes 6291460
  146.2 3.6 %copy-start.3 = (bf16[384,2048]{1,0:T(8,128)(2,1)S(1)}, bf16[384,2048]{1,0:T(8,128)(2,1)}, u32[]{:S(2)}) copy-start(bf16[384,2048]{1,0:T(8,128)(2,1)} %get-tuple-element.30) | copy-start | bytes 4718596
